TPU v7x, 32 devices: a whole 2x2x4 slice. The times are simulated.
32 devices in a mesh: ep: 8 (over z, x), tp: 4 (over y, core).
Axes of the slice: x: 2, y: 2, z: 4, core: 2. Of those that a mesh axis runs over, the one named last changes fastest.
Arguments:
- memory_query_matrix: bfloat16 [4096, 1024], P('ep', 'tp'), may hold values from -0.59765625 to 2
- memory_key_matrix: bfloat16 [4096, 1024], P('ep', 'tp'), may hold values from -0.59765625 to 2
- memory_value_matrix: bfloat16 [4096, 1024], P('ep', 'tp'), may hold values from -6 to 6
- input_gate_logits: float32 [4, 4096], P('tp', 'ep'), may hold values from -6 to 260
- forget_gate_logits: float32 [4, 4096], P('tp', 'ep'), may hold values from -1 to 20
- forget_log_boosts: float32 [4, 4096], P('tp', 'ep'), may hold values from -0.7 to 0
- head_norm_scale: float32 [1024], P('tp'), may hold values from 0.1 to 1.9
- memory_output_matrix: bfloat16 [1024, 2048], replicated, may hold values from -0.1875 to 0.1875
- projection_norm_scale: float32 [2048], replicated, may hold values from 0.1 to 1.9
- second_batch_rows: bfloat16 [6144, 2048], P(('ep', 'tp')), may hold values from -6 to 6
- expert_prenorm_scale: float32 [2048], replicated, may hold values from 0.1 to 1.9
- selected_expert_index: int32 [6144, 2], P(('ep', 'tp')), may hold values from 0 to 7, all different within a row; in each aligned block of 192 rows (0 to 191, 192 to 383, ...) at most 96 rows name the same one
- group_route_probability: float32 [6144], P(('ep', 'tp')), may hold values from 0.2 to 1
- expert_choice_scores: float32 [6144, 2], P(('ep', 'tp')), may hold values from -6 to 6
- expert_gate_matrix: bfloat16 [8, 2048, 512], P('ep'), may hold values from -0.125 to 0.125
- expert_up_matrix: bfloat16 [8, 2048, 512], P('ep'), may hold values from -0.125 to 0.125
- expert_down_matrix: bfloat16 [8, 512, 2048], P('ep'), may hold values from -0.25 to 0.25
Outputs:
- mixed_rows: bfloat16 [4096, 2048], P(('ep', 'tp'))
- routed_rows: bfloat16 [6144, 2048], P(('ep', 'tp'))
Inputs may be any that keep to these rules, and one draw needn't show every extreme that they name: `selected_expert_index`: each row names 2 different experts; among the rows of one device no expert is named more than 96 times, and in some device one expert is named exactly that often.
All inputs are finite; a program needn't handle non-finite values.
Results may differ from a plain program's by a relative error of at most 0.013.
Values may be sent and summed in bfloat16 or wider, within the bound.
A program may use at most 128 MiB of HBM per device.

v0:
```python
import jax
import jax.numpy as jnp
from jax import lax
from jax.sharding import PartitionSpec as P

SPAN = 128
floor_log = -1e30
norm_eps = 1e-06
exact = lax.Precision.HIGHEST


def entering_2(array, axis, combine, identity):
    devices, position = (lax.axis_size(axis), lax.axis_index(axis))
    everything = jax.tree.map(lambda part: lax.all_gather(part, axis), array)
    start = jax.tree.map(
        lambda part, zero: jnp.broadcast_to(jnp.asarray(zero, part.dtype), part.shape),
        array,
        identity,
    )

    def step(k, before):
        reached = k < position
        new = combine(before, jax.tree.map(lambda part: part[k], everything))
        return jax.tree.map(lambda a, b: jnp.where(reached, a, b), new, before)

    return lax.fori_loop(0, devices, step, start)


def rms_scale(values, gain):
    squares = jnp.mean(values * values, axis=-1, keepdims=True)
    return values * lax.rsqrt(squares + norm_eps) * gain


def span_step(carry, inputs):
    memory, normer, stabil = carry
    query, keyrow, valrow, in_gate, log_retain_factor = inputs
    key_scale = query.shape[-1] ** (-0.5)
    length = query.shape[1]
    causal = jnp.tril(jnp.ones((length, length), dtype=bool))
    cumulative = jnp.cumsum(log_retain_factor, axis=-1)
    decay_map = cumulative[:, :, None] - cumulative[:, None, :] + in_gate[:, None, :]
    decay_map = jnp.where(causal[None], decay_map, -jnp.inf)
    carried = cumulative + stabil[:, None]
    peak = jnp.maximum(carried, jnp.max(decay_map, axis=-1))
    within = jnp.exp(decay_map - peak[:, :, None])
    across = jnp.exp(carried - peak)
    products = jnp.einsum("htd,hsd->hts", query, keyrow, preferred_element_type=jnp.float32)
    scores = products * key_scale * within
    qfloat = query.astype(jnp.float32)
    denominator = jnp.sum(scores, axis=-1) + across * jnp.einsum(
        "hd,htd->ht", normer, qfloat, precision=exact
    )
    weights = scores.astype(jnp.bfloat16)
    numerator = jnp.einsum("hts,hsd->htd", weights, valrow, preferred_element_type=jnp.float32)
    numerator = numerator + across[:, :, None] * jnp.einsum(
        "hed,htd->hte", memory, qfloat, precision=exact
    )
    output = numerator / jnp.maximum(jnp.abs(denominator), jnp.exp(-peak))[:, :, None]
    span_end = cumulative[:, -1]
    gap_log = span_end[:, None] - cumulative + in_gate
    new_peak = jnp.maximum(span_end + stabil, jnp.max(gap_log, axis=-1))
    shrink = jnp.exp(span_end + stabil - new_peak)
    spread = jnp.exp(gap_log - new_peak[:, None]) * key_scale
    keys_weighted = keyrow.astype(jnp.float32) * spread[:, :, None]
    memory = shrink[:, None, None] * memory + jnp.einsum(
        "hse,hsd->hed", valrow.astype(jnp.float32), keys_weighted, precision=exact
    )
    normer = shrink[:, None] * normer + jnp.sum(keys_weighted, axis=1)
    return ((memory, normer, new_peak), output)


def span_summary(keyrow, valrow, in_gate, log_retain_factor):
    key_scale = keyrow.shape[-1] ** (-0.5)
    cumulative = jnp.cumsum(log_retain_factor, axis=-1)
    span_end = cumulative[:, -1]
    gap_log = span_end[:, None] - cumulative + in_gate
    peak = jnp.max(gap_log, axis=-1)
    spread = jnp.exp(gap_log - peak[:, None]) * key_scale
    keys_weighted = keyrow.astype(jnp.float32) * spread[:, :, None]
    memory = jnp.einsum("hse,hsd->hed", valrow.astype(jnp.float32), keys_weighted, precision=exact)
    return (span_end, peak, memory, jnp.sum(keys_weighted, axis=1))


def join_states(earlier, later):
    total_early, peak_early, memory_early, normer_early = earlier
    total_late, peak_late, memory_late, normer_late = later
    peak = jnp.maximum(total_late + peak_early, peak_late)
    factor_early = jnp.exp(total_late + peak_early - peak)
    factor_late = jnp.exp(peak_late - peak)
    memory = factor_early[:, None, None] * memory_early + factor_late[:, None, None] * memory_late
    normer = factor_early[:, None] * normer_early + factor_late[:, None] * normer_late
    return (total_early + total_late, peak, memory, normer)


def shards(
    memory_query_matrix,
    memory_key_matrix,
    memory_value_matrix,
    input_gate_logits,
    forget_gate_logits,
    forget_log_boosts,
    head_norm_scale,
    memory_output_matrix,
    projection_norm_scale,
    second_batch_rows,
    expert_prenorm_scale,
    selected_expert_index,
    group_route_probability,
    expert_choice_scores,
    expert_gate_matrix,
    expert_up_matrix,
    expert_down_matrix,
):
    local_heads = input_gate_logits.shape[0]
    positions = input_gate_logits.shape[1]
    head_size = memory_query_matrix.shape[1] // local_heads
    spans = positions // SPAN

    def by_head(rows):
        return rows.reshape(positions, local_heads, head_size).transpose(1, 0, 2)

    def to_spans(values):
        shaped = values.reshape((local_heads, spans, SPAN) + values.shape[2:])
        return jnp.moveaxis(shaped, 1, 0)

    query = by_head(memory_query_matrix)
    keyrow = by_head(memory_key_matrix)
    valrow = by_head(memory_value_matrix)
    log_retain_factor = jax.nn.log_sigmoid(forget_gate_logits) + forget_log_boosts
    summary = span_summary(keyrow, valrow, input_gate_logits, log_retain_factor)
    neutral = (
        jnp.zeros((local_heads,), jnp.float32),
        jnp.full((local_heads,), floor_log, jnp.float32),
        jnp.zeros((local_heads, head_size, head_size), jnp.float32),
        jnp.zeros((local_heads, head_size), jnp.float32),
    )
    entering = entering_2(summary, "ep", join_states, neutral)
    start = (entering[2], entering[3], entering[1])
    inputs = (
        to_spans(query),
        to_spans(keyrow),
        to_spans(valrow),
        to_spans(input_gate_logits),
        to_spans(log_retain_factor),
    )
    _, cells = lax.scan(span_step, start, inputs)
    cells = jnp.moveaxis(cells, 0, 1).reshape(local_heads, positions, head_size)
    scaled = (cells * head_norm_scale.reshape(local_heads, 1, head_size)).astype(jnp.bfloat16)
    head_out = scaled.transpose(1, 0, 2).reshape(positions, local_heads * head_size)
    first_row = lax.axis_index("tp") * head_out.shape[1]
    weight_rows = lax.dynamic_slice_in_dim(memory_output_matrix, first_row, head_out.shape[1], 0)
    projected = lax.psum_scatter(
        jnp.dot(head_out, weight_rows, preferred_element_type=jnp.float32).astype(jnp.bfloat16),
        "tp",
        scatter_dimension=0,
        tiled=True,
    ).astype(jnp.float32)
    mixed_rows = rms_scale(projected, projection_norm_scale).astype(jnp.bfloat16)
    token_count = second_batch_rows.shape[0]
    choices_per = selected_expert_index.shape[1]
    experts = lax.axis_size("ep")
    capacity = 2 * choices_per * token_count // experts
    ffn_rows = rms_scale(second_batch_rows.astype(jnp.float32), expert_prenorm_scale).astype(
        jnp.bfloat16
    )
    flat_ids = selected_expert_index.reshape(-1)
    onehot = (flat_ids[:, None] == jnp.arange(experts, dtype=jnp.int32)[None, :]).astype(jnp.int32)
    rank = jnp.sum((jnp.cumsum(onehot, axis=0) - onehot) * onehot, axis=1)
    slot = flat_ids * capacity + rank
    placing = (jnp.arange(experts * capacity, dtype=jnp.int32)[:, None] == slot[None, :]).astype(
        jnp.bfloat16
    )
    placing = jnp.sum(placing.reshape(experts * capacity, token_count, choices_per), axis=-1)
    outgoing = jnp.dot(placing, ffn_rows, preferred_element_type=jnp.float32).astype(jnp.bfloat16)
    outgoing = outgoing.reshape(experts, capacity, ffn_rows.shape[1])
    w_gate = expert_gate_matrix[0]
    w_up = expert_up_matrix[0]
    w_down = expert_down_matrix[0]
    received = lax.all_to_all(outgoing, "ep", split_axis=0, concat_axis=0, tiled=True)
    flat_rows = received.reshape(-1, received.shape[2])
    gate = jnp.dot(flat_rows, w_gate, preferred_element_type=jnp.float32)
    upper = jnp.dot(flat_rows, w_up, preferred_element_type=jnp.float32)
    hidden = (jax.nn.silu(gate) * upper).astype(jnp.bfloat16)
    answer = jnp.dot(hidden, w_down, preferred_element_type=jnp.float32).astype(jnp.bfloat16)
    answers = answer.reshape(received.shape)
    back = lax.all_to_all(answers, "ep", split_axis=0, concat_axis=0, tiled=True)
    picked = back.reshape(experts * capacity, back.shape[2])[slot].reshape(
        token_count, choices_per, back.shape[2]
    )
    route_weight = group_route_probability[:, None] * jax.nn.softmax(expert_choice_scores, axis=-1)
    routed_rows = jnp.sum(route_weight[:, :, None] * picked.astype(jnp.float32), axis=1).astype(
        jnp.bfloat16
    )
    return (mixed_rows, routed_rows)


def solution(mesh):
    return jax.shard_map(
        shards,
        mesh=mesh,
        in_specs=(
            P("ep", "tp"),
            P("ep", "tp"),
            P("ep", "tp"),
            P("tp", "ep"),
            P("tp", "ep"),
            P("tp", "ep"),
            P("tp"),
            P(),
            P(),
            P(("ep", "tp"), None),
            P(),
            P(("ep", "tp"), None),
            P(("ep", "tp")),
            P(("ep", "tp"), None),
            P("ep", None, None),
            P("ep", None, None),
            P("ep", None, None),
        ),
        out_specs=(P(("ep", "tp"), None), P(("ep", "tp"), None)),
        check_vma=False,
    )
```

profile of v0, /device:TPU:0, one launch (start us, length us, event | category | flops | bytes accessed | tf_op | source)
XLA Modules:
  0.0 327.3 jit_solution(2145870936360990207)
XLA Ops:
  9.6 2.0 fusion.76
  11.5 1.9 exponential_multiply_fusion.1
  13.5 2.4 convolution_bitcast_fusion.2
  19.1 1.3 bitcast_dynamic-update-slice_fusion
  20.5 1.3 dynamic-update-slice.1
  22.2 2.8 convolution_convert_fusion.1
  25.0 7.4 %all-to-all-start = ((bf16[8,96,2048]{2,1,0:T(8,128)(2,1)}), bf16[8,96,2048]{2,1,0:T(8,128)(2,1)}, u32[]{:S(2)}, u32[]{:S(2)}) async-start(bf16[8,96,2048]{2,1,0:T(8,128)(2,1)} %bitcast.221), calls=%async_computation.1 | async-start | bytes 6291456 | tf_op jit(solution)/shard_map/all_to_all | solution.py:179
  32.5 86.9 %all-reduce.2 = (f32[8]{0:T(128)S(1)}, f32[8]{0:T(128)S(1)}) all-reduce(f32[8]{0:T(128)S(1)} %bitcast_dynamic-update-slice_fusion, f32[8]{0:T(128)S(1)} %dynamic-update-slice.1), channel_id=1, replica_groups=mesh['ep'=8,'tp'=4] {'ep'}, use_global_device_ids=true, to_apply=%add | all-reduce | flops 16 | bytes 128
  119.5 32.2 %all-gather.2 = f32[8,1,256]{2,1,0:T(1,128)S(1)} all-gather(f32[1,1,256]{2,1,0:T(1,128)S(1)} %bitcast.240), channel_id=3, replica_groups=mesh['ep'=8,'tp'=4] {'ep'}, dimensions={0}, use_global_device_ids=true | all-gather | bytes 9216 | tf_op jit(solution)/shard_map/all_gather | solution.py:14
  151.7 2.9 copy.38
  154.6 29.8 %while.35 = (s32[]{:T(128)}, f32[1]{0:T(128)}, f32[1,256,256]{2,1,0:T(8,128)S(1)}, f32[1,256]{1,0:T(1,128)S(1)}, s32[]{:T(128)}, /*index=5*/f32[8,1]{0,1:T(1,128...) while((s32[]{:T(128)}, f32[1]{0:T(128)}, ...), condition=%wide.region_5.6_spmd.clone, body=%wide.region_4.5_spmd.clone.sunk | while | flops 328969 | bytes 789756 | solution.py:26
  160.9 1.1 fusion.121
  184.5 33.1 %while.34 = (s32[]{:T(128)}, f32[1,256,256]{2,1,0:T(8,128)S(1)}, f32[1,256]{1,0:T(1,128)S(1)}, f32[1]{0:T(128)}, f32[4,1,128,256]{3,2,1,0:T(8,128)S(1)}, /*index...) while((s32[]{:T(128)}, f32[1,256,256]{2,1,0:T(8,128)S(1)}, ...), condition=%wide.region_12.13_spmd, body=%wide.region_6.12_spmd.sunk | while | flops 219137792 | bytes 1794273 | solution.py:146
  185.4 1.3 fusion.113
  190.9 1.2 fusion.120
  193.7 1.3 fusion.113
  199.2 1.2 fusion.120
  201.9 1.3 fusion.113
  207.5 1.2 fusion.120
  210.2 1.3 fusion.113
  215.8 1.2 fusion.120
  217.6 5.5 %fusion.46 = f32[768,512]{1,0:T(8,128)} fusion(bf16[768,2048]{1,0:T(8,128)(2,1)} %bitcast.46, bf16[1,2048,512]{2,1,0:T(8,128)(2,1)} %param.35), kind=kOutput, calls=%fused_computation.71 | convolution fusion | flops 1610612736 | bytes 6815744 | tf_op jit(solution)/shard_map/dot_general | solution.py:181
  223.1 8.2 %convolution_convert_fusion = bf16[768,2048]{1,0:T(8,128)(2,1)} fusion(bf16[1,512,2048]{2,1,0:T(8,128)(2,1)S(1)} %copy-done, f32[768,512]{1,0:T(8,128)} %fusion.46, bf16[768,2048]{1,0:T(8,128)(2,1)} %bitcast.46, bf16[1,2048,512]{2,1,0:T(8,128)(2,1)} %param.36), kind=kOutput, calls=%fused_computation.64 | convolution fusion | flops 3225157632 | bytes 12058624 | tf_op jit(solution)/shard_map/dot_general | solution.py:184
  231.3 4.6 %all-to-all-start.1 = ((bf16[8,96,2048]{2,1,0:T(8,128)(2,1)}), bf16[8,96,2048]{2,1,0:T(8,128)(2,1)}, u32[]{:S(2)}, u32[]{:S(2)}) async-start(bf16[8,96,2048]{2,1,0:T(8,128)(2,1)} %bitcast.225), calls=%async_computation.2 | async-start | bytes 6291456 | tf_op jit(solution)/shard_map/all_to_all | solution.py:186
  236.1 3.3 %convolution_convert_fusion.2 = bf16[512,2048]{1,0:T(8,128)(2,1)} fusion(bf16[512,256]{1,0:T(8,128)(2,1)S(1)} %fusion.64, bf16[1024,2048]{1,0:T(8,128)(2,1)} %param.28, s32[]{:T(128)S(6)} %select_n.82), kind=kOutput, calls=%fused_computation.67 | convolution fusion | flops 537919488 | bytes 3407876 | tf_op jit(solution)/shard_map/dot_general | solution.py:153
  240.3 31.5 %reduce-scatter.2.cloned.1.call-done = bf16[128,2048]{1,0:T(8,128)(2,1)} async-done(((bf16[512,2048]{1,0:T(8,128)(2,1)}), bf16[128,2048]{1,0:T(8,128)(2,1)}) %reduce-scatter.2.cloned.1.call-update) | async-done | bytes 524304 | tf_op jit(solution)/shard_map/reduce_scatter | solution.py:152
  271.9 1.2 fusion.54
  273.1 2.0 fusion.56
  275.2 25.4 %all-to-all-done.1 = bf16[8,96,2048]{2,1,0:T(8,128)(2,1)} async-done(((bf16[8,96,2048]{2,1,0:T(8,128)(2,1)}), bf16[8,96,2048]{2,1,0:T(8,128)(2,1)}, u32[]{:S(2)}, u32[]{:S(2)}) %all-to-all-start.1) | async-done | bytes 3145760 | tf_op jit(solution)/shard_map/all_to_all | solution.py:186
  300.6 7.3 %gather_fusion = bf16[384,2048]{1,0:T(8,128)(2,1)} fusion(bf16[768,2048]{1,0:T(8,128)(2,1)} %bitcast.51, s32[1024]{0:T(1024)S(1)} %pad_clamp_fusion), kind=kCustom, calls=%fused_computation | custom fusion | bytes 3147264 | tf_op jit(solution)/shard_map/gather | solution.py:187
  307.9 4.7 %reshape.522 = f32[192,2,2048]{2,1,0:T(2,128)} reshape(bf16[384,2048]{1,0:T(8,128)(2,1)} %gather_fusion) | data formatting | bytes 4718592 | tf_op jit(solution)/shard_map/convert_element_type | solution.py:191
  312.7 7.8 %multiply_reduce_fusion = bf16[192,2048]{1,0:T(8,128)(2,1)} fusion(f32[192,2,2048]{2,1,0:T(2,128)} %reshape.522, f32[192,2]{1,0:T(8,128)S(1)} %copy.33), kind=kLoop, calls=%fused_computation.66 | loop fusion | flops 1179648 | bytes 3933696 | tf_op jit(solution)/shard_map/reduce_sum | solution.py:191
  (137 shorter events, 37.8 us)
Async XLA Ops:
  7.2 215.9 %copy-start = (bf16[1,512,2048]{2,1,0:T(8,128)(2,1)S(1)}, bf16[1,512,2048]{2,1,0:T(8,128)(2,1)}, u32[]{:S(2)}) copy-start(bf16[1,512,2048]{2,1,0:T(8,128)(2,1)} %param.37) | copy-start | bytes 6291460
  7.2 11.3 %copy-start.10 = (u32[32]{0:T(128)S(1)}, u32[32]{0:T(128)}, u32[]{:S(2)}) copy-start(u32[32]{0:T(128)} %constant.112) | copy-start | bytes 388
  7.2 14.8 %copy-start.3 = (bf16[192,2048]{1,0:T(8,128)(2,1)S(1)}, bf16[192,2048]{1,0:T(8,128)(2,1)}, u32[]{:S(2)}) copy-start(bf16[192,2048]{1,0:T(8,128)(2,1)} %param.30) | copy-start | bytes 2359300
  7.2 15.0 %copy-start.6 = (f32[2048]{0:T(1024)S(1)}, f32[2048]{0:T(1024)}, u32[]{:S(2)}) copy-start(f32[2048]{0:T(1024)} %param.31) | copy-start | bytes 24580
  7.2 144.5 %all-gather.5.cloned.1.call-start = ((), (), s32[]{:S(2)}) async-start(), calls=%async_computation.4 | async-start | bytes 2359296 | tf_op jit(solution)/shard_map/all_gather | solution.py:14
  25.0 94.3 %copy-start.1 = (bf16[512,256]{1,0:T(8,128)(2,1)S(1)}, bf16[512,256]{1,0:T(8,128)(2,1)}, u32[]{:S(2)}) copy-start(bf16[512,256]{1,0:T(8,128)(2,1)} %param.22) | copy-start | bytes 786436
  25.0 192.6 %all-to-all-start = ((bf16[8,96,2048]{2,1,0:T(8,128)(2,1)}), bf16[8,96,2048]{2,1,0:T(8,128)(2,1)}, u32[]{:S(2)}, u32[]{:S(2)}) async-start(bf16[8,96,2048]{2,1,0:T(8,128)(2,1)} %bitcast.221), calls=%async_computation.1 | async-start | bytes 6291456 | tf_op jit(solution)/shard_map/all_to_all | solution.py:179
  154.6 29.8 %copy-start.2 = (bf16[512,256]{1,0:T(8,128)(2,1)S(1)}, bf16[512,256]{1,0:T(8,128)(2,1)}, u32[]{:S(2)}) copy-start(bf16[512,256]{1,0:T(8,128)(2,1)} %param.23) | copy-start | bytes 786436
  154.6 29.8 %copy-start.4 = (f32[1,512]{1,0:T(1,128)S(1)}, f32[1,512]{1,0:T(1,128)}, u32[]{:S(2)}) copy-start(f32[1,512]{1,0:T(1,128)} %param.24) | copy-start | bytes 6148
  231.3 4.8 %copy-start.8 = (f32[256]{0:T(256)S(1)}, f32[256]{0:T(256)}, u32[]{:S(2)}) copy-start(f32[256]{0:T(256)} %param.27) | copy-start | bytes 3076
  231.3 69.3 %all-to-all-start.1 = ((bf16[8,96,2048]{2,1,0:T(8,128)(2,1)}), bf16[8,96,2048]{2,1,0:T(8,128)(2,1)}, u32[]{:S(2)}, u32[]{:S(2)}) async-start(bf16[8,96,2048]{2,1,0:T(8,128)(2,1)} %bitcast.225), calls=%async_computation.2 | async-start | bytes 6291456 | tf_op jit(solution)/shard_map/all_to_all | solution.py:186
  235.8 36.0 %reduce-scatter.2.cloned.1.call-start = ((), (), s32[]{:S(2)}) async-start(), calls=%async_computation.3 | async-start | bytes 2621440 | tf_op jit(solution)/shard_map/reduce_scatter | solution.py:152
  239.4 0.7 copy-start.5
  239.4 0.7 copy-start.9
  239.4 33.7 %copy-start.7 = (f32[2048]{0:T(1024)S(1)}, f32[2048]{0:T(1024)}, u32[]{:S(2)}) copy-start(f32[2048]{0:T(1024)} %param.29) | copy-start | bytes 24580
Sparse Core Ops, SparseCore 0:
  16.0 102.3 all-gather.4
  239.6 32.2 reduce-scatter.1
where the time goes:
time: 329 us; the launch traced here: 327 us
  blocking collectives  119 us (36%)
  waiting for transfers between devices  57 us (17%)
  matrix products  37.5 us (11%)
  other arithmetic  37.2 us (11%)
  local copies, waits for them, and re-layouts  28.6 us (9%)
  loops' own time  21.4 us (7%)
  between operations  14.3 us (4%)
  starting transfers between devices  12.2 us (4%)
    unnamed x1, blocking collectives  86.9 us
    all_gather x1, blocking collectives, entering_2(): everything = jax.tree.map(lambda part: lax.all_gather(part, axis), array)  32.2 us
    reduce_scatter x1, waiting for transfers between devices, shards(): lax.psum_scatter(jnp.dot(head_out, weight_rows, preferred_element_type=jn...  31.5 us
    all_to_all x1, waiting for transfers between devices, shards(): lax.all_to_all(answers, 'ep', split_axis=0, concat_axis=0, tiled=True)  25.4 us
    another operation x1, loops' own time, entering_2(): return lax.fori_loop(0, devices, step, start)  15.8 us
    select_n x16, other arithmetic, step(): return jax.tree.map(lambda a, b: jnp.where(reached, a, b), new, before)  9.28 us
    dot_general x1, matrix products, shards(): jnp.dot(hidden, w_down, preferred_element_type=jnp.float32)  8.18 us
    reduce_sum x1, other arithmetic, shards(): jnp.sum(route_weight[:, :, None] * picked.astype(jnp.float32), axis=1)  7.76 us
  transfers between devices with their start and end apart: 4, of which 2 were waited for; matrix products, arithmetic and copies ran while one was open for 19% of the time, Pallas kernels for 0%

commit v1 on v0

--- a/solution.py
+++ b/solution.py
@@ -7,6 +7,18 @@
 floor_log = -1e30
 norm_eps = 1e-06
 exact = lax.Precision.HIGHEST
+
+
+def in_blocks(x, dim, size):
+    shape = x.shape
+    tiles = x.reshape(*shape[:dim], size, shape[dim] // size, *shape[dim + 1 :])
+    return jnp.moveaxis(tiles, dim, 0)
+
+
+def joined_along(parts, dim):
+    dims = list(parts.shape[1:])
+    dims[dim] *= parts.shape[0]
+    return jnp.moveaxis(parts, 0, dim).reshape(dims)
 
 
 def entering_2(array, axis, combine, identity):
@@ -183,7 +195,15 @@
     hidden = (jax.nn.silu(gate) * upper).astype(jnp.bfloat16)
     answer = jnp.dot(hidden, w_down, preferred_element_type=jnp.float32).astype(jnp.bfloat16)
     answers = answer.reshape(received.shape)
-    back = lax.all_to_all(answers, "ep", split_axis=0, concat_axis=0, tiled=True)
+    size, mine = (lax.axis_size("ep"), lax.axis_index("ep"))
+    blocks = in_blocks(answers, 0, size)
+    out = blocks
+    for turn in range(1, size):
+        target, source = ((mine + turn) % size, (mine - turn) % size)
+        sent = lax.dynamic_index_in_dim(blocks, target, 0)
+        other = lax.ppermute(sent, "ep", [(i, (i + turn) % size) for i in range(size)])
+        out = lax.dynamic_update_slice_in_dim(out, other, source, axis=0)
+    back = joined_along(out, 0)
     picked = back.reshape(experts * capacity, back.shape[2])[slot].reshape(
         token_count, choices_per, back.shape[2]
     )

time: 329 us -> 343 us (1.043)
  the two profiles are of different devices: /device:TPU:0 before, /device:TPU:10 now
where the time goes in v1:
time: 343 us; the launch traced here: 341 us
  blocking collectives  113 us (33%)
  waiting for transfers between devices  55.3 us (16%)
  local copies, waits for them, and re-layouts  39.4 us (11%)
  other arithmetic  38.3 us (11%)
  matrix products  37.9 us (11%)
  starting transfers between devices  21.9 us (6%)
  loops' own time  21.1 us (6%)
  between operations  14.5 us (4%)
    unnamed x1, blocking collectives  97.5 us
    ppermute x7, waiting for transfers between devices, shards(): lax.ppermute(sent, 'ep', [(i, (i + turn) % size) for i in range(size)])  55.3 us
    another operation x1, loops' own time, entering_2(): return lax.fori_loop(0, devices, step, start)  15.8 us
    ppermute x7, starting transfers between devices, shards(): lax.ppermute(sent, 'ep', [(i, (i + turn) % size) for i in range(size)])  15.5 us
    all_gather x1, blocking collectives, entering_2(): everything = jax.tree.map(lambda part: lax.all_gather(part, axis), array)  15 us
    select_n x16, other arithmetic, step(): return jax.tree.map(lambda a, b: jnp.where(reached, a, b), new, before)  9.29 us
    dot_general x1, matrix products, shards(): jnp.dot(hidden, w_down, preferred_element_type=jnp.float32)  8.54 us
    reduce_sum x1, other arithmetic, shards(): jnp.sum(route_weight[:, :, None] * picked.astype(jnp.float32), axis=1)  7.76 us
  transfers between devices with their start and end apart: 10, of which 6 were waited for; matrix products, arithmetic and copies ran while one was open for 30% of the time, Pallas kernels for 0%

profile of v1, /device:TPU:10, one launch (start us, length us, event | category | flops | bytes accessed | tf_op | source)
XLA Modules:
  0.0 340.9 jit_solution(13842055114552490688)
XLA Ops:
  9.6 2.0 fusion.76
  11.5 1.9 exponential_multiply_fusion.1
  13.5 2.4 convolution_bitcast_fusion.2
  19.7 1.4 bitcast_dynamic-update-slice_fusion
  21.1 1.3 dynamic-update-slice.1
  22.6 1.4 fusion.48
  24.0 2.8 convolution_convert_fusion.1
  26.8 6.4 %all-to-all-start = ((bf16[8,96,2048]{2,1,0:T(8,128)(2,1)}), bf16[8,96,2048]{2,1,0:T(8,128)(2,1)}, u32[]{:S(2)}, u32[]{:S(2)}) async-start(bf16[8,96,2048]{2,1,0:T(8,128)(2,1)} %bitcast.224), calls=%async_computation.1 | async-start | bytes 6291456 | tf_op jit(solution)/shard_map/all_to_all | solution.py:191
  33.2 97.5 %all-reduce.2 = (f32[8]{0:T(128)S(1)}, f32[8]{0:T(128)S(1)}) all-reduce(f32[8]{0:T(128)S(1)} %bitcast_dynamic-update-slice_fusion, f32[8]{0:T(128)S(1)} %dynamic-update-slice.1), channel_id=1, replica_groups=mesh['ep'=8,'tp'=4] {'ep'}, use_global_device_ids=true, to_apply=%add | all-reduce | flops 16 | bytes 128
  130.9 15.0 %all-gather.2 = f32[8,1,256]{2,1,0:T(1,128)S(1)} all-gather(f32[1,1,256]{2,1,0:T(1,128)S(1)} %bitcast.242), channel_id=3, replica_groups=mesh['ep'=8,'tp'=4] {'ep'}, dimensions={0}, use_global_device_ids=true | all-gather | bytes 9216 | tf_op jit(solution)/shard_map/all_gather | solution.py:26
  145.9 2.9 copy.38
  148.8 29.8 %while.35 = (s32[]{:T(128)}, f32[1]{0:T(128)}, f32[1,256,256]{2,1,0:T(8,128)S(1)}, f32[1,256]{1,0:T(1,128)S(1)}, s32[]{:T(128)}, /*index=5*/f32[8,1]{0,1:T(1,128...) while((s32[]{:T(128)}, f32[1]{0:T(128)}, ...), condition=%wide.region_5.6_spmd.clone, body=%wide.region_4.5_spmd.clone.sunk | while | flops 328969 | bytes 789756 | solution.py:38
  178.6 32.8 %while.34 = (s32[]{:T(128)}, f32[1,256,256]{2,1,0:T(8,128)S(1)}, f32[1,256]{1,0:T(1,128)S(1)}, f32[1]{0:T(128)}, f32[4,1,128,256]{3,2,1,0:T(8,128)S(1)}, /*index...) while((s32[]{:T(128)}, f32[1,256,256]{2,1,0:T(8,128)S(1)}, ...), condition=%wide.region_12.13_spmd, body=%wide.region_6.12_spmd.sunk | while | flops 219137792 | bytes 1794273 | solution.py:158
  179.6 1.3 fusion.113
  211.5 3.3 convolution_convert_fusion.2
  214.8 5.6 %fusion.46 = f32[768,512]{1,0:T(8,128)} fusion(bf16[768,2048]{1,0:T(8,128)(2,1)} %bitcast.46, bf16[1,2048,512]{2,1,0:T(8,128)(2,1)} %param.35), kind=kOutput, calls=%fused_computation.71 | convolution fusion | flops 1610612736 | bytes 6815744 | tf_op jit(solution)/shard_map/dot_general | solution.py:193
  220.4 8.5 %convolution_convert_fusion = bf16[768,2048]{1,0:T(8,128)(2,1)} fusion(bf16[1,512,2048]{2,1,0:T(8,128)(2,1)S(1)} %copy-done, f32[768,512]{1,0:T(8,128)} %fusion.46, bf16[768,2048]{1,0:T(8,128)(2,1)} %bitcast.46, bf16[1,2048,512]{2,1,0:T(8,128)(2,1)} %param.36), kind=kOutput, calls=%fused_computation.64 | convolution fusion | flops 3225157632 | bytes 12058624 | tf_op jit(solution)/shard_map/dot_general | solution.py:196
  231.1 7.2 %collective-permute-done = bf16[1,1,96,2048]{3,2,0,1:T(8,128)(2,1)} collective-permute-done((bf16[1,1,96,2048]{3,2,0,1:T(8,128)(2,1)S(1)}, bf16[1,1,96,2048]{3,2,0,1:T(8,128)(2,1)}, u32[]{:S(2)}, u32[]{:S(2)}) %collective-permute-start) | collective-permute-done | bytes 393248 | tf_op jit(solution)/shard_map/ppermute | solution.py:204
  238.3 3.0 constant_dynamic-slice_fusion.4
  242.4 11.9 %collective-permute-start.2 = (bf16[1,1,96,2048]{3,2,0,1:T(8,128)(2,1)}, bf16[1,1,96,2048]{3,2,0,1:T(8,128)(2,1)}, u32[]{:S(2)}, u32[]{:S(2)}) collective-permute-start(bf16[1,1,96,2048]{3,2,0,1:T(8,128)(2,1)} %get-tuple-element.332), channel_id=1, source_target_pairs={{0,12},{4,16},{8,20},{12,24},{16,28},{20,0},{24,4},{28,8},{1,13},{... | collective-permute-start | bytes 1179656 | tf_op jit(solution)/shard_map/ppermute | solution.py:204
  254.7 1.5 collective-permute-start.5
  256.2 29.0 %collective-permute-done.1 = bf16[1,1,96,2048]{3,2,0,1:T(8,128)(2,1)} collective-permute-done((bf16[1,1,96,2048]{3,2,0,1:T(8,128)(2,1)}, bf16[1,1,96,2048]{3,2,0,1:T(8,128)(2,1)}, u32[]{:S(2)}, u32[]{:S(2)}) %collective-permute-start.1) | collective-permute-done | bytes 393248 | tf_op jit(solution)/shard_map/ppermute | solution.py:204
  285.2 1.8 constant_dynamic-update-slice_fusion.5
  287.0 6.1 %collective-permute-done.2 = bf16[1,1,96,2048]{3,2,0,1:T(8,128)(2,1)} collective-permute-done((bf16[1,1,96,2048]{3,2,0,1:T(8,128)(2,1)}, bf16[1,1,96,2048]{3,2,0,1:T(8,128)(2,1)}, u32[]{:S(2)}, u32[]{:S(2)}) %collective-permute-start.2) | collective-permute-done | bytes 393248 | tf_op jit(solution)/shard_map/ppermute | solution.py:204
  293.1 1.8 constant_dynamic-update-slice_fusion.4
  294.9 2.4 collective-permute-done.3
  298.9 3.1 collective-permute-done.5
  302.7 7.4 %collective-permute-done.6 = bf16[1,1,96,2048]{3,2,0,1:T(8,128)(2,1)S(1)} collective-permute-done((bf16[1,1,96,2048]{3,2,0,1:T(8,128)(2,1)S(1)}, bf16[1,1,96,2048]{3,2,0,1:T(8,128)(2,1)S(1)}, u32[]{:S(2)}, u32[]{:S(2)}) %collective-permute-start.6) | collective-permute-done | bytes 393248 | tf_op jit(solution)/shard_map/ppermute | solution.py:204
  311.0 7.3 %gather_fusion = bf16[384,2048]{1,0:T(8,128)(2,1)} fusion(bf16[768,2048]{1,0:T(8,128)(2,1)} %bitcast.223, s32[1024]{0:T(1024)S(1)} %pad_clamp_fusion), kind=kCustom, calls=%fused_computation | custom fusion | bytes 3147264 | tf_op jit(solution)/shard_map/gather | solution.py:207
  318.3 4.7 %reshape.514 = f32[192,2,2048]{2,1,0:T(2,128)} reshape(bf16[384,2048]{1,0:T(8,128)(2,1)} %gather_fusion) | data formatting | bytes 4718592 | tf_op jit(solution)/shard_map/convert_element_type | solution.py:211
  323.0 7.8 %multiply_reduce_fusion = bf16[192,2048]{1,0:T(8,128)(2,1)} fusion(f32[192,2,2048]{2,1,0:T(2,128)} %reshape.514, f32[192,2]{1,0:T(8,128)S(1)} %copy.33), kind=kLoop, calls=%fused_computation.66 | loop fusion | flops 1179648 | bytes 3933696 | tf_op jit(solution)/shard_map/reduce_sum | solution.py:211
  332.0 2.0 fusion.56
  (155 shorter events, 54.7 us)
Async XLA Ops:
  7.2 213.2 %copy-start = (bf16[1,512,2048]{2,1,0:T(8,128)(2,1)S(1)}, bf16[1,512,2048]{2,1,0:T(8,128)(2,1)}, u32[]{:S(2)}) copy-start(bf16[1,512,2048]{2,1,0:T(8,128)(2,1)} %param.37) | copy-start | bytes 6291460
  7.2 16.8 %copy-start.3 = (bf16[192,2048]{1,0:T(8,128)(2,1)S(1)}, bf16[192,2048]{1,0:T(8,128)(2,1)}, u32[]{:S(2)}) copy-start(bf16[192,2048]{1,0:T(8,128)(2,1)} %param.30) | copy-start | bytes 2359300
  7.2 16.8 %copy-start.6 = (f32[2048]{0:T(1024)S(1)}, f32[2048]{0:T(1024)}, u32[]{:S(2)}) copy-start(f32[2048]{0:T(1024)} %param.31) | copy-start | bytes 24580
  7.2 138.7 %all-gather.5.cloned.1.call-start = ((), (), s32[]{:S(2)}) async-start(), calls=%async_computation.3 | async-start | bytes 2359296 | tf_op jit(solution)/shard_map/all_gather | solution.py:26
  26.8 103.9 %copy-start.1 = (bf16[512,256]{1,0:T(8,128)(2,1)S(1)}, bf16[512,256]{1,0:T(8,128)(2,1)}, u32[]{:S(2)}) copy-start(bf16[512,256]{1,0:T(8,128)(2,1)} %param.22) | copy-start | bytes 786436
  26.8 188.0 %all-to-all-start = ((bf16[8,96,2048]{2,1,0:T(8,128)(2,1)}), bf16[8,96,2048]{2,1,0:T(8,128)(2,1)}, u32[]{:S(2)}, u32[]{:S(2)}) async-start(bf16[8,96,2048]{2,1,0:T(8,128)(2,1)} %bitcast.224), calls=%async_computation.1 | async-start | bytes 6291456 | tf_op jit(solution)/shard_map/all_to_all | solution.py:191
  33.2 297.6 %reduce-scatter.2.cloned.1.call-start = ((), (), s32[]{:S(2)}) async-start(), calls=%async_computation.2 | async-start | bytes 2621440 | tf_op jit(solution)/shard_map/reduce_scatter | solution.py:164
  148.8 29.8 %copy-start.2 = (bf16[512,256]{1,0:T(8,128)(2,1)S(1)}, bf16[512,256]{1,0:T(8,128)(2,1)}, u32[]{:S(2)}) copy-start(bf16[512,256]{1,0:T(8,128)(2,1)} %param.23) | copy-start | bytes 786436
  148.8 29.8 %copy-start.4 = (f32[1,512]{1,0:T(1,128)S(1)}, f32[1,512]{1,0:T(1,128)}, u32[]{:S(2)}) copy-start(f32[1,512]{1,0:T(1,128)} %param.24) | copy-start | bytes 6148
  178.6 32.8 %copy-start.8 = (f32[256]{0:T(256)S(1)}, f32[256]{0:T(256)}, u32[]{:S(2)}) copy-start(f32[256]{0:T(256)} %param.27) | copy-start | bytes 3076
  220.4 10.7 %copy-start.5 = (f32[192,2]{0,1:T(2,128)S(1)}, f32[192,2]{0,1:T(2,128)}, u32[]{:S(2)}) copy-start(f32[192,2]{0,1:T(2,128)} %param.34) | copy-start | bytes 4612
  228.9 13.4 %copy-start.9 = (f32[192]{0:T(256)S(1)}, f32[192]{0:T(256)}, u32[]{:S(2)}) copy-start(f32[192]{0:T(256)} %param.33) | copy-start | bytes 2308
  230.0 8.4 %collective-permute-start = (bf16[1,1,96,2048]{3,2,0,1:T(8,128)(2,1)S(1)}, bf16[1,1,96,2048]{3,2,0,1:T(8,128)(2,1)}, u32[]{:S(2)}, u32[]{:S(2)}) collective-permute-start(bf16[1,1,96,2048]{3,2,0,1:T(8,128)(2,1)S(1)} %constant_dynamic-slice_fusion.10), channel_id=1, source_target_pairs={{0,4},{4,8},{8,12},{12,16},{16,20},{20,24},{24,28},{28,0},{1,5},{5... | collective-permute-start | bytes 1179656 | tf_op jit(solution)/shard_map/ppermute | solution.py:204
  241.3 43.9 %collective-permute-start.1 = (bf16[1,1,96,2048]{3,2,0,1:T(8,128)(2,1)}, bf16[1,1,96,2048]{3,2,0,1:T(8,128)(2,1)}, u32[]{:S(2)}, u32[]{:S(2)}) collective-permute-start(bf16[1,1,96,2048]{3,2,0,1:T(8,128)(2,1)} %get-tuple-element.333), channel_id=1, source_target_pairs={{0,8},{4,12},{8,16},{12,20},{16,24},{20,28},{24,0},{28,4},{1,9},{5... | collective-permute-start | bytes 1179656 | tf_op jit(solution)/shard_map/ppermute | solution.py:204
  242.4 50.7 %collective-permute-start.2 = (bf16[1,1,96,2048]{3,2,0,1:T(8,128)(2,1)}, bf16[1,1,96,2048]{3,2,0,1:T(8,128)(2,1)}, u32[]{:S(2)}, u32[]{:S(2)}) collective-permute-start(bf16[1,1,96,2048]{3,2,0,1:T(8,128)(2,1)} %get-tuple-element.332), channel_id=1, source_target_pairs={{0,12},{4,16},{8,20},{12,24},{16,28},{20,0},{24,4},{28,8},{1,13},{... | collective-permute-start | bytes 1179656 | tf_op jit(solution)/shard_map/ppermute | solution.py:204
  254.6 42.7 %collective-permute-start.3 = (bf16[1,1,96,2048]{3,2,0,1:T(8,128)(2,1)}, bf16[1,1,96,2048]{3,2,0,1:T(8,128)(2,1)S(1)}, u32[]{:S(2)}, u32[]{:S(2)}) collective-permute-start(bf16[1,1,96,2048]{3,2,0,1:T(8,128)(2,1)} %get-tuple-element.331), channel_id=1, source_target_pairs={{0,16},{4,20},{8,24},{12,28},{16,0},{20,4},{24,8},{28,12},{1,17},{... | collective-permute-start | bytes 1179656 | tf_op jit(solution)/shard_map/ppermute | solution.py:204
  254.7 43.4 %collective-permute-start.4 = (bf16[1,1,96,2048]{3,2,0,1:T(8,128)(2,1)S(1)}, bf16[1,1,96,2048]{3,2,0,1:T(8,128)(2,1)S(1)}, u32[]{:S(2)}, u32[]{:S(2)}) collective-permute-start(bf16[1,1,96,2048]{3,2,0,1:T(8,128)(2,1)S(1)} %get-tuple-element.330), channel_id=1, source_target_pairs={{0,20},{4,24},{8,28},{12,0},{16,4},{20,8},{24,12},{28,16},{1,21},{... | collective-permute-start | bytes 1179656 | tf_op jit(solution)/shard_map/ppermute | solution.py:204
  254.7 47.2 %collective-permute-start.5 = (bf16[1,1,96,2048]{3,2,0,1:T(8,128)(2,1)S(1)}, bf16[1,1,96,2048]{3,2,0,1:T(8,128)(2,1)S(1)}, u32[]{:S(2)}, u32[]{:S(2)}) collective-permute-start(bf16[1,1,96,2048]{3,2,0,1:T(8,128)(2,1)S(1)} %get-tuple-element.329), channel_id=1, source_target_pairs={{0,24},{4,28},{8,0},{12,4},{16,8},{20,12},{24,16},{28,20},{1,25},{... | collective-permute-start | bytes 1179656 | tf_op jit(solution)/shard_map/ppermute | solution.py:204
  285.2 24.9 %collective-permute-start.6 = (bf16[1,1,96,2048]{3,2,0,1:T(8,128)(2,1)S(1)}, bf16[1,1,96,2048]{3,2,0,1:T(8,128)(2,1)S(1)}, u32[]{:S(2)}, u32[]{:S(2)}) collective-permute-start(bf16[1,1,96,2048]{3,2,0,1:T(8,128)(2,1)S(1)} %get-tuple-element.328), channel_id=1, source_target_pairs={{0,28},{4,0},{8,4},{12,8},{16,12},{20,16},{24,20},{28,24},{1,29},{... | collective-permute-start | bytes 1179656 | tf_op jit(solution)/shard_map/ppermute | solution.py:204
  323.0 9.0 %copy-start.7 = (f32[2048]{0:T(1024)S(1)}, f32[2048]{0:T(1024)}, u32[]{:S(2)}) copy-start(f32[2048]{0:T(1024)} %param.29) | copy-start | bytes 24580
Sparse Core Ops, SparseCore 0:
  16.0 93.0 all-gather.4
  214.9 32.7 reduce-scatter.1
